TPU v7x, 32 devices: a whole 2x2x4 slice. The times are simulated.
32 devices in a mesh: grp: 2 (over x), ep: 16 (over z, y, core).
Axes of the slice: x: 2, y: 2, z: 4, core: 2. Of those that a mesh axis runs over, the one named last changes fastest.
Arguments:
- sequence_input_rows: bfloat16 [224, 2048], P(('grp', 'ep')), parts along dimension 0, may hold values from -6 to 6
- value_key_state: float32 [224, 32, 64, 64], P(('grp', 'ep')), parts along dimension 0, may hold values from -4 to 4
- receptance_matrix: bfloat16 [2048, 2048], P(None, 'ep'), may hold values from -0.125 to 0.125
- key_matrix: bfloat16 [2048, 2048], P(None, 'ep'), may hold values from -0.125 to 0.125
- value_matrix: bfloat16 [2048, 2048], P(None, 'ep'), may hold values from -0.125 to 0.125
- decay_lowrank_input: bfloat16 [2048, 64], replicated, may hold values from -0.125 to 0.125
- decay_lowrank_output: bfloat16 [64, 2048], replicated, may hold values from -0.75 to 0.75
- decay_base_preact: float32 [2048], replicated, may hold values from -6 to -1
- context_rate_input: bfloat16 [2048, 64], replicated, may hold values from -0.125 to 0.125
- context_rate_output: bfloat16 [64, 2048], replicated, may hold values from -0.75 to 0.75
- context_rate_base: float32 [2048], replicated, may hold values from -4 to 4
- removal_key_scale: float32 [2048], replicated, may hold values from 0.1 to 1.9
- key_context_rate_blend: float32 [2048], replicated, may hold values from 0.1 to 1.9
- present_item_coefficient: float32 [32, 64], replicated, may hold values from -0.9 to 0.9
- head_norm_gain: float32 [2048], replicated, may hold values from 0.1 to 1.9
- mixer_output_matrix: bfloat16 [2048, 2048], P(None, 'ep'), may hold values from -0.125 to 0.125
- mixer_norm_gain: float32 [2048], replicated, may hold values from 0.1 to 1.9
- group_router_columns: bfloat16 [2048, 4], replicated, may hold values from -8 to 8
- expert_router_columns: bfloat16 [2048, 16], replicated, may hold values from -0.125 to 0.125
- expert_gate_matrix: bfloat16 [16, 2048, 256], P('ep'), may hold values from -0.125 to 0.125
- expert_up_matrix: bfloat16 [16, 2048, 256], P('ep'), may hold values from -0.125 to 0.125
- expert_down_matrix: bfloat16 [16, 256, 2048], P('ep'), may hold values from -0.375 to 0.375
- final_norm_gain: float32 [2048], replicated, may hold values from 0.1 to 1.9
- routes: int32 [224, 4], P(('grp', 'ep')), parts along dimension 0, may hold values from 0 to 15, as said below
Outputs:
- tokens_out: bfloat16 [224, 2048], P(('grp', 'ep')), parts along dimension 0
- next_recurrent_state: float32 [224, 32, 64, 64], P(('grp', 'ep')), parts along dimension 0
There are 2 independent parts, one for each index of `grp`. A program takes and returns all parts, laid end to end along the dimension named above; an argument that names none is the same for every part. Nothing has to cross between parts.
Inputs may be any that keep to these rules, and one draw needn't show every extreme that they name: `routes`: the 4 experts of a row are different and lie in the same group (expert // 4). In each aligned block of 7 rows (the rows of one device) no expert is named more than 2 times, and in every block some expert is named exactly 2 times.
All inputs are finite; a program needn't handle non-finite values.
Results may differ from a plain program's by a relative error of at most 0.0067.
Values may be sent and summed in bfloat16 or wider, within the bound.
A program may use at most 128 MiB of HBM per device.

v0:
```python
import jax
import jax.numpy as jnp
from jax import lax
from jax.sharding import PartitionSpec as P

CAP = 2
residual_scale = 8.0**0.25
norm_eps = 1e-05
group_eps = 0.00064


def layer_norm(values, norm_gain):
    center = jnp.mean(values, -1, keepdims=True)
    spread = jnp.mean(jnp.square(values - center), -1, keepdims=True)
    return (values - center) * lax.rsqrt(spread + norm_eps) * norm_gain


def token_mixer_step(
    sequence_input_rows,
    receptance_rows,
    key_projected_rows,
    value_projected_rows,
    value_key_state,
    decay_lowrank_input,
    decay_lowrank_output,
    decay_base_preact,
    context_rate_input,
    context_rate_output,
    context_rate_base,
    removal_key_scale,
    key_context_rate_blend,
    present_item_coefficient,
    head_norm_gain,
):
    series_entry_number = sequence_input_rows.shape[0]
    attention_subspace_number, subspace_dimension = present_item_coefficient.shape
    decay_low = jnp.tanh(
        jnp.dot(sequence_input_rows, decay_lowrank_input, preferred_element_type=jnp.float32)
    ).astype(jnp.bfloat16)
    decay_pre = decay_base_preact + jnp.dot(
        decay_low, decay_lowrank_output, preferred_element_type=jnp.float32
    )
    log_rate = -jax.nn.softplus(-decay_pre) - 0.5
    decay = jnp.exp(-jnp.exp(log_rate))
    iclr_low = jnp.dot(
        sequence_input_rows, context_rate_input, preferred_element_type=jnp.float32
    ).astype(jnp.bfloat16)
    iclr_rate = jax.nn.sigmoid(
        context_rate_base
        + jnp.dot(iclr_low, context_rate_output, preferred_element_type=jnp.float32)
    )

    def to_heads(values):
        return values.astype(jnp.float32).reshape(
            series_entry_number, attention_subspace_number, subspace_dimension
        )

    acceptance_subspaces = to_heads(receptance_rows)
    key_heads = to_heads(key_projected_rows)
    content_subspace_entries = to_heads(value_projected_rows)
    decay_heads = to_heads(decay)
    rate_heads = to_heads(iclr_rate)
    scaled_key = key_heads * removal_key_scale.reshape(
        attention_subspace_number, subspace_dimension
    )
    removal_dir = scaled_key * lax.rsqrt(
        jnp.sum(scaled_key * scaled_key, -1, keepdims=True) + 1e-06
    )
    adjusted_lookup_vector = key_heads * (
        1.0
        + (rate_heads - 1.0)
        * key_context_rate_blend.reshape(attention_subspace_number, subspace_dimension)
    )
    removed = jnp.einsum(
        "bhvk,bhk->bhv", value_key_state, removal_dir, precision=lax.Precision.HIGHEST
    )
    next_recurrent_state = (
        value_key_state * decay_heads[:, :, None, :]
        - removed[..., None] * (removal_dir * rate_heads)[:, :, None, :]
        + content_subspace_entries[..., None] * adjusted_lookup_vector[:, :, None, :]
    )
    readout = jnp.einsum(
        "bhvk,bhk->bhv", next_recurrent_state, acceptance_subspaces, precision=lax.Precision.HIGHEST
    )
    center = jnp.mean(readout, -1, keepdims=True)
    spread = jnp.mean(jnp.square(readout - center), -1, keepdims=True)
    standardized_entries = (
        (readout - center)
        * lax.rsqrt(spread + group_eps)
        * head_norm_gain.reshape(attention_subspace_number, subspace_dimension)
    )
    present_extra_reward = (
        jnp.sum(
            acceptance_subspaces * adjusted_lookup_vector * present_item_coefficient,
            -1,
            keepdims=True,
        )
        * content_subspace_entries
    )
    attention_mixing_outcome = (
        (standardized_entries + present_extra_reward)
        .reshape(series_entry_number, attention_subspace_number * subspace_dimension)
        .astype(jnp.bfloat16)
    )
    return (attention_mixing_outcome, next_recurrent_state)


def routing_gate(hidden, route_rows, chosen, group_router_columns, expert_router_columns):
    group_count = group_router_columns.shape[1]
    expert_count = expert_router_columns.shape[1]
    per_group = expert_count // group_count
    group_logits = jnp.dot(hidden, group_router_columns, preferred_element_type=jnp.float32)
    expert_logits = jnp.dot(hidden, expert_router_columns, preferred_element_type=jnp.float32)
    largest = jnp.max(group_logits, -1, keepdims=True)
    lifted = jnp.exp(group_logits - largest)
    in_group = (chosen // per_group)[:, None] == jnp.arange(group_count, dtype=jnp.int32)[None, :]
    group_prob = jnp.sum(jnp.where(in_group, lifted, 0.0), -1) / jnp.sum(lifted, -1)
    columns = jnp.arange(expert_count, dtype=jnp.int32)[None, :]
    chosen_logit = jnp.sum(jnp.where(chosen[:, None] == columns, expert_logits, 0.0), -1)
    total = jnp.zeros_like(chosen_logit)
    for slot in range(route_rows.shape[1]):
        other_logit = jnp.sum(
            jnp.where(route_rows[:, slot][:, None] == columns, expert_logits, 0.0), -1
        )
        total = total + jnp.exp(other_logit - chosen_logit)
    return group_prob / total


def expert_mlp(inputs, expert_weights):
    gate_weight, up_weight, down_weight = expert_weights
    gate_part = jnp.dot(inputs, gate_weight[0], preferred_element_type=jnp.float32)
    up_part = jnp.dot(inputs, up_weight[0], preferred_element_type=jnp.float32)
    act = (jax.nn.silu(gate_part) * up_part).astype(jnp.bfloat16)
    return jnp.dot(act, down_weight[0], preferred_element_type=jnp.float32).astype(jnp.bfloat16)


def by_exchange(hidden, routes, routers, expert_weights):
    series_entry_number, model_width = hidden.shape
    expert_count = routers[1].shape[1]
    is_named = routes[:, :, None] == jnp.arange(expert_count, dtype=jnp.int32)[None, None, :]
    per_row = jnp.sum(is_named.astype(jnp.int32), 1)
    before = jnp.cumsum(per_row, 0) - per_row
    slot_rank = jnp.sum(jnp.where(is_named, before[:, None, :], 0), -1)
    slot_index = routes * CAP + slot_rank
    placing = (
        slot_index[:, :, None] == jnp.arange(expert_count * CAP, dtype=jnp.int32)[None, None, :]
    ).astype(jnp.bfloat16)
    outgoing = jnp.einsum("rks,rd->sd", placing, hidden, preferred_element_type=jnp.float32)
    outgoing = outgoing.astype(jnp.bfloat16).reshape(expert_count, CAP, model_width)
    incoming = lax.all_to_all(outgoing, "ep", split_axis=0, concat_axis=0, tiled=True)
    flat_rows = incoming.reshape(-1, model_width)
    finished = expert_mlp(flat_rows, expert_weights).reshape(incoming.shape)
    returned = lax.all_to_all(finished, "ep", split_axis=0, concat_axis=0, tiled=True).reshape(
        expert_count * CAP, model_width
    )
    gate_values = jnp.stack(
        [
            routing_gate(hidden, routes, routes[:, slot], routers[0], routers[1])
            for slot in range(routes.shape[1])
        ],
        1,
    )
    picked = returned[slot_index]
    return jnp.sum(gate_values[:, :, None] * picked.astype(jnp.float32), 1)


def on_device(
    sequence_input_rows,
    value_key_state,
    receptance_matrix,
    key_matrix,
    value_matrix,
    decay_lowrank_input,
    decay_lowrank_output,
    decay_base_preact,
    context_rate_input,
    context_rate_output,
    context_rate_base,
    removal_key_scale,
    key_context_rate_blend,
    present_item_coefficient,
    head_norm_gain,
    mixer_output_matrix,
    mixer_norm_gain,
    group_router_columns,
    expert_router_columns,
    expert_gate_matrix,
    expert_up_matrix,
    expert_down_matrix,
    final_norm_gain,
    routes,
):
    section = lax.all_gather(sequence_input_rows, "ep", axis=0, tiled=True)
    columns = [
        jnp.dot(section, weight, preferred_element_type=jnp.float32).astype(jnp.bfloat16)
        for weight in (receptance_matrix, key_matrix, value_matrix)
    ]
    projected = jnp.stack(columns, axis=1)
    own_heads = lax.all_to_all(projected, "ep", split_axis=0, concat_axis=2, tiled=True)
    attention_mixing_outcome, next_recurrent_state = token_mixer_step(
        sequence_input_rows,
        own_heads[:, 0],
        own_heads[:, 1],
        own_heads[:, 2],
        value_key_state,
        decay_lowrank_input,
        decay_lowrank_output,
        decay_base_preact,
        context_rate_input,
        context_rate_output,
        context_rate_base,
        removal_key_scale,
        key_context_rate_blend,
        present_item_coefficient,
        head_norm_gain,
    )
    out_columns = jnp.dot(
        lax.all_gather(attention_mixing_outcome, "ep", axis=0, tiled=True),
        mixer_output_matrix,
        preferred_element_type=jnp.float32,
    ).astype(jnp.bfloat16)
    attn_out = lax.all_to_all(out_columns, "ep", split_axis=0, concat_axis=1, tiled=True)
    hidden = layer_norm(
        residual_scale * sequence_input_rows.astype(jnp.float32) + attn_out.astype(jnp.float32),
        mixer_norm_gain,
    ).astype(jnp.bfloat16)
    expert_weights = (expert_gate_matrix, expert_up_matrix, expert_down_matrix)
    routers = (group_router_columns, expert_router_columns)
    expert_sum = by_exchange(hidden, routes, routers, expert_weights)
    tokens_out = layer_norm(
        residual_scale * hidden.astype(jnp.float32) + expert_sum, final_norm_gain
    ).astype(jnp.bfloat16)
    return (tokens_out, next_recurrent_state)


def solution(mesh):
    in_specs = (
        P(("grp", "ep"), None),
        P(("grp", "ep"), None, None, None),
        P(None, "ep"),
        P(None, "ep"),
        P(None, "ep"),
        P(),
        P(),
        P(),
        P(),
        P(),
        P(),
        P(),
        P(),
        P(),
        P(),
        P(None, "ep"),
        P(),
        P(),
        P(),
        P("ep", None, None),
        P("ep", None, None),
        P("ep", None, None),
        P(),
        P(("grp", "ep"), None),
    )
    out_specs = (P(("grp", "ep"), None), P(("grp", "ep"), None, None, None))
    return jax.shard_map(
        on_device, mesh=mesh, in_specs=in_specs, out_specs=out_specs, check_vma=False
    )
```

profile of v0, /device:TPU:0, one launch (start us, length us, event | category | flops | bytes accessed | tf_op | source)
XLA Modules:
  0.0 138.3 jit_solution(8020242776843022416)
XLA Ops:
  0.6 25.0 %all-gather = bf16[16,7,2048]{2,1,0:T(8,128)(2,1)S(1)} all-gather(bf16[1,7,2048]{2,1,0:T(8,128)(2,1)} %bitcast.101), channel_id=1, replica_groups=mesh['grp'=2,'ep'=16] {'ep'}, dimensions={0}, use_global_device_ids=true | all-gather | bytes 487424 | tf_op jit(solution)/shard_map/all_gather | solution.py:193
  25.6 0.2 reshape.474
  25.8 1.3 fusion.10
  27.1 1.3 fusion.11
  28.4 1.3 fusion.9
  29.7 0.7 copy.40
  30.4 3.5 %all-to-all-start = ((bf16[112,3,128]{2,1,0:T(4,128)(2,1)}), bf16[112,3,128]{2,1,0:T(4,128)(2,1)S(1)}, u32[]{:S(2)}, u32[]{:S(2)}) async-start(bf16[112,3,128]{2,1,0:T(4,128)(2,1)} %copy.40), calls=%async_computation | async-start | bytes 229376 | tf_op jit(solution)/shard_map/all_to_all | solution.py:199
  34.0 0.8 copy.43
  34.9 0.3 select_reduce_fusion
  35.1 1.4 %fusion.4 = f32[7,2048]{1,0:T(8,128)S(1)} fusion(bf16[64,2048]{1,0:T(8,128)(2,1)} %param.33, bf16[7,2048]{1,0:T(8,128)(2,1)} %param.24, bf16[2048,64]{0,1:T(8,128)(2,1)} %param.32, f32[2048]{0:T(1024)} %param.34), kind=kOutput, calls=%fused_computation.9 | convolution fusion | flops 3727808 | bytes 618496 | tf_op jit(solution)/shard_map/dot_general | solution.py:50
  36.6 1.5 %fusion.24 = f32[7,2048]{1,0:T(8,128)S(1)} fusion(bf16[64,2048]{1,0:T(8,128)(2,1)} %param.30, bf16[7,2048]{1,0:T(8,128)(2,1)} %param.24, bf16[2048,64]{0,1:T(8,128)(2,1)} %param.29, f32[2048]{0:T(1024)} %param.31), kind=kOutput, calls=%fused_computation.45 | convolution fusion | flops 3828160 | bytes 618496 | tf_op jit(solution)/shard_map/dot_general | solution.py:40
  38.1 0.8 slice_bitcast_fusion.2
  38.9 0.8 mul.214
  39.8 0.8 mul.225
  40.6 0.8 mul.233
  41.9 0.1 multiply_reduce_fusion.2
  42.2 13.6 %fusion.48 = f32[7,32,1,64]{3,2,1,0:T(1,128)S(1)} fusion(f32[7,32,64,1]{2,3,1,0:T(1,128)S(1)} %bitcast.104, f32[7,32,64,64]{3,2,1,0:T(8,128)} %param.25), kind=kOutput, calls=%fused_computation.134 | convolution fusion | flops 11010048 | bytes 3784704 | tf_op jit(solution)/shard_map/bhvk,bhk->bhv/dot_general | solution.py:74
  55.9 7.9 %multiply_add_fusion = f32[7,32,64,64]{3,2,1,0:T(8,128)S(1)} fusion(f32[7,32,64,64]{3,2,1,0:T(8,128)} %param.25, f32[7,32,64]{2,1,0:T(8,128)S(1)} %get-tuple-element.15, f32[7,32,64]{2,1,0:T(8,128)S(1)} %reshape.448, f32[7,32,64]{2,1,0:T(8,128)S(1)} %get-tuple-element.13, f32[7,32,64]{2,1,0:T(8,128)S(1)} %bitcast.103, f32[7,32,64]{2,1,0:T(8,128)S(1)} %mul.211), kind=kLoop, calls=%fused_computation.2 | loop fusion | flops 4587520 | bytes 7626752 | tf_op jit(solution)/shard_map/add | solution.py:78
  63.8 3.0 %copy-done.1 = f32[7,32,64,64]{3,2,1,0:T(8,128)} copy-done((f32[7,32,64,64]{3,2,1,0:T(8,128)}, f32[7,32,64,64]{3,2,1,0:T(8,128)S(1)}, u32[]{:S(2)}) %copy-start.1) | copy-done | bytes 3670040
  66.9 5.8 %fusion.49 = f32[7,32,1,64]{3,2,1,0:T(1,128)S(1)} fusion(f32[7,32,64,64]{3,2,1,0:T(8,128)S(1)} %multiply_add_fusion, bf16[7,32,64,1]{2,3,1,0:T(2,128)(2,1)S(1)} %reshape.483), kind=kOutput, calls=%fused_computation.135 | convolution fusion | flops 11010048 | bytes 3756032 | tf_op jit(solution)/shard_map/bhvk,bhk->bhv/dot_general | solution.py:82
  72.7 0.1 reduce_sum.203
  72.8 0.2 multiply_reduce_fusion.1
  73.0 0.5 fusion.8
  73.5 0.1 reshape.475
  73.6 23.2 %all-gather.1 = bf16[16,7,2048]{2,1,0:T(8,128)(2,1)S(1)} all-gather(bf16[1,7,2048]{2,1,0:T(8,128)(2,1)S(1)} %reshape.475), channel_id=1, replica_groups=mesh['grp'=2,'ep'=16] {'ep'}, dimensions={0}, use_global_device_ids=true | all-gather | bytes 487424 | tf_op jit(solution)/shard_map/all_gather | solution.py:218
  96.8 0.2 reshape.476
  97.0 1.3 convolution_convert_fusion.2
  98.3 0.6 all_to_all.33
  98.9 3.5 %all-to-all-start.1 = ((bf16[16,7,128]{2,1,0:T(8,128)(2,1)}), bf16[16,7,128]{2,1,0:T(8,128)(2,1)S(1)}, u32[]{:S(2)}, u32[]{:S(2)}) async-start(bf16[16,7,128]{2,1,0:T(8,128)(2,1)} %all_to_all.33), calls=%async_computation.1 | async-start | bytes 65536 | tf_op jit(solution)/shard_map/all_to_all | solution.py:222
  102.4 6.6 %all-to-all-done.1 = bf16[16,7,128]{2,1,0:T(8,128)(2,1)S(1)} async-done(((bf16[16,7,128]{2,1,0:T(8,128)(2,1)}), bf16[16,7,128]{2,1,0:T(8,128)(2,1)S(1)}, u32[]{:S(2)}, u32[]{:S(2)}) %all-to-all-start.1) | async-done | bytes 28704 | tf_op jit(solution)/shard_map/all_to_all | solution.py:222
  109.0 0.1 fusion.26
  109.2 0.2 multiply_reduce_fusion.4
  109.5 0.2 fusion.50
  109.7 0.7 reshape.443
  110.4 3.5 %all-to-all-start.2 = ((bf16[16,2,2048]{2,1,0:T(2,128)(2,1)}), bf16[16,2,2048]{2,1,0:T(2,128)(2,1)S(1)}, u32[]{:S(2)}, u32[]{:S(2)}) async-start(bf16[16,2,2048]{2,1,0:T(2,128)(2,1)} %reshape.443), calls=%async_computation.2 | async-start | bytes 262144 | tf_op jit(solution)/shard_map/all_to_all | solution.py:150
  114.0 0.1 fusion.47
  114.2 0.3 select_reduce_fusion.4
  114.4 7.4 %all-to-all-done.2 = bf16[16,2,2048]{2,1,0:T(2,128)(2,1)S(1)} async-done(((bf16[16,2,2048]{2,1,0:T(2,128)(2,1)}), bf16[16,2,2048]{2,1,0:T(2,128)(2,1)S(1)}, u32[]{:S(2)}, u32[]{:S(2)}) %all-to-all-start.2) | async-done | bytes 131104 | tf_op jit(solution)/shard_map/all_to_all | solution.py:150
  121.9 1.5 %fusion.17 = f32[32,256]{1,0:T(8,128)S(1)} fusion(bf16[32,2048]{1,0:T(8,128)(2,1)S(1)} %reshape.444, bf16[1,2048,256]{2,1,0:T(8,128)(2,1)} %param.43), kind=kOutput, calls=%fused_computation.29 | convolution fusion | flops 33554432 | bytes 1212416 | tf_op jit(solution)/shard_map/dot_general | solution.py:131
  123.4 0.7 convolution_convert_fusion
  124.1 0.8 reshape.445
  124.9 3.5 %all-to-all-start.3 = ((bf16[16,2,2048]{2,1,0:T(2,128)(2,1)}), bf16[16,2,2048]{2,1,0:T(2,128)(2,1)S(1)}, u32[]{:S(2)}, u32[]{:S(2)}) async-start(bf16[16,2,2048]{2,1,0:T(2,128)(2,1)} %reshape.445), calls=%async_computation.3 | async-start | bytes 262144 | tf_op jit(solution)/shard_map/all_to_all | solution.py:153
  128.6 7.7 %all-to-all-done.3 = bf16[16,2,2048]{2,1,0:T(2,128)(2,1)S(1)} async-done(((bf16[16,2,2048]{2,1,0:T(2,128)(2,1)}), bf16[16,2,2048]{2,1,0:T(2,128)(2,1)S(1)}, u32[]{:S(2)}, u32[]{:S(2)}) %all-to-all-start.3) | async-done | bytes 131104 | tf_op jit(solution)/shard_map/all_to_all | solution.py:153
  136.3 0.6 gather_fusion
  137.1 0.2 multiply_reduce_fusion
  137.3 0.1 fusion.32
  137.4 0.2 multiply_reduce_fusion.3
  137.6 0.7 multiply_convert_fusion
  (50 shorter events, 1.5 us)
Async XLA Ops:
  0.6 122.8 %copy-start = (bf16[1,256,2048]{2,1,0:T(8,128)(2,1)S(1)}, bf16[1,256,2048]{2,1,0:T(8,128)(2,1)}, u32[]{:S(2)}) copy-start(bf16[1,256,2048]{2,1,0:T(8,128)(2,1)} %param.45) | copy-start | bytes 3145732
  30.4 11.1 %all-to-all-start = ((bf16[112,3,128]{2,1,0:T(4,128)(2,1)}), bf16[112,3,128]{2,1,0:T(4,128)(2,1)S(1)}, u32[]{:S(2)}, u32[]{:S(2)}) async-start(bf16[112,3,128]{2,1,0:T(4,128)(2,1)} %copy.40), calls=%async_computation | async-start | bytes 229376 | tf_op jit(solution)/shard_map/all_to_all | solution.py:199
  63.8 3.1 %copy-start.1 = (f32[7,32,64,64]{3,2,1,0:T(8,128)}, f32[7,32,64,64]{3,2,1,0:T(8,128)S(1)}, u32[]{:S(2)}) copy-start(f32[7,32,64,64]{3,2,1,0:T(8,128)S(1)} %multiply_add_fusion) | copy-start | bytes 11010052
  66.8 6.2 %copy-start.4 = (f32[32,64]{1,0:T(8,128)S(1)}, f32[32,64]{1,0:T(8,128)}, u32[]{:S(2)}) copy-start(f32[32,64]{1,0:T(8,128)} %param.37) | copy-start | bytes 24580
  66.8 42.2 %copy-start.2 = (bf16[7,2048]{1,0:T(8,128)(2,1)S(1)}, bf16[7,2048]{1,0:T(8,128)(2,1)}, u32[]{:S(2)}) copy-start(bf16[7,2048]{1,0:T(8,128)(2,1)} %param.24) | copy-start | bytes 86020
  66.8 42.5 %copy-start.6 = (f32[2048]{0:T(1024)S(1)}, f32[2048]{0:T(1024)}, u32[]{:S(2)}) copy-start(f32[2048]{0:T(1024)} %param.40) | copy-start | bytes 24580
  66.8 47.1 %copy-start.8 = (bf16[2048,4]{0,1:T(4,128)(2,1)S(1)}, bf16[2048,4]{0,1:T(4,128)(2,1)}, u32[]{:S(2)}) copy-start(bf16[2048,4]{0,1:T(4,128)(2,1)} %param.41) | copy-start | bytes 49156
  66.8 47.3 %copy-start.7 = (bf16[2048,16]{0,1:T(8,128)(2,1)S(1)}, bf16[2048,16]{0,1:T(8,128)(2,1)}, u32[]{:S(2)}) copy-start(bf16[2048,16]{0,1:T(8,128)(2,1)} %param.42) | copy-start | bytes 196612
  66.9 56.5 %copy-start.3 = (bf16[1,2048,256]{2,1,0:T(8,128)(2,1)S(1)}, bf16[1,2048,256]{2,1,0:T(8,128)(2,1)}, u32[]{:S(2)}) copy-start(bf16[1,2048,256]{2,1,0:T(8,128)(2,1)} %param.44) | copy-start | bytes 3145732
  72.7 65.0 %copy-start.5 = (f32[2048]{0:T(1024)S(1)}, f32[2048]{0:T(1024)}, u32[]{:S(2)}) copy-start(f32[2048]{0:T(1024)} %param.46) | copy-start | bytes 24580
  98.9 10.1 %all-to-all-start.1 = ((bf16[16,7,128]{2,1,0:T(8,128)(2,1)}), bf16[16,7,128]{2,1,0:T(8,128)(2,1)S(1)}, u32[]{:S(2)}, u32[]{:S(2)}) async-start(bf16[16,7,128]{2,1,0:T(8,128)(2,1)} %all_to_all.33), calls=%async_computation.1 | async-start | bytes 65536 | tf_op jit(solution)/shard_map/all_to_all | solution.py:222
  110.4 11.4 %all-to-all-start.2 = ((bf16[16,2,2048]{2,1,0:T(2,128)(2,1)}), bf16[16,2,2048]{2,1,0:T(2,128)(2,1)S(1)}, u32[]{:S(2)}, u32[]{:S(2)}) async-start(bf16[16,2,2048]{2,1,0:T(2,128)(2,1)} %reshape.443), calls=%async_computation.2 | async-start | bytes 262144 | tf_op jit(solution)/shard_map/all_to_all | solution.py:150
  124.9 11.4 %all-to-all-start.3 = ((bf16[16,2,2048]{2,1,0:T(2,128)(2,1)}), bf16[16,2,2048]{2,1,0:T(2,128)(2,1)S(1)}, u32[]{:S(2)}, u32[]{:S(2)}) async-start(bf16[16,2,2048]{2,1,0:T(2,128)(2,1)} %reshape.445), calls=%async_computation.3 | async-start | bytes 262144 | tf_op jit(solution)/shard_map/all_to_all | solution.py:153
where the time goes:
time: 139 us; the launch traced here: 138 us
  blocking collectives  48.2 us (35%)
  matrix products  30.5 us (22%)
  waiting for transfers between devices  21.7 us (16%)
  starting transfers between devices  14 us (10%)
  other arithmetic  12 us (9%)
  local copies, waits for them, and re-layouts  11 us (8%)
    all_gather x1, blocking collectives, on_device(): section = lax.all_gather(sequence_input_rows, 'ep', axis=0, tiled=True)  25 us
    all_gather x1, blocking collectives, on_device(): lax.all_gather(attention_mixing_outcome, 'ep', axis=0, tiled=True)  23.2 us
    dot_general x1, matrix products, token_mixer_step(): jnp.einsum('bhvk,bhk->bhv', value_key_state, removal_dir, precision=lax.P...  13.6 us
    add x1, other arithmetic, token_mixer_step(): value_key_state * decay_heads[:, :, None, :]  7.89 us
    all_to_all x1, waiting for transfers between devices, by_exchange(): lax.all_to_all(finished, 'ep', split_axis=0, concat_axis=0, tiled=True)  7.72 us
    all_to_all x1, waiting for transfers between devices, by_exchange(): lax.all_to_all(outgoing, 'ep', split_axis=0, concat_axis=0, tiled=True)  7.39 us
    all_to_all x1, waiting for transfers between devices, on_device(): lax.all_to_all(out_columns, 'ep', split_axis=0, concat_axis=1, tiled=True)  6.58 us
    dot_general x1, matrix products, token_mixer_step(): jnp.einsum('bhvk,bhk->bhv', next_recurrent_state, acceptance_subspaces, p...  5.79 us
  transfers between devices with their start and end apart: 4, of which 3 were waited for; matrix products, arithmetic and copies ran while one was open for 6% of the time, Pallas kernels for 0%

commit v1 on v0

--- a/solution.py
+++ b/solution.py
@@ -219,7 +219,12 @@
         mixer_output_matrix,
         preferred_element_type=jnp.float32,
     ).astype(jnp.bfloat16)
-    attn_out = lax.all_to_all(out_columns, "ep", split_axis=0, concat_axis=1, tiled=True)
+    attn_out = jnp.concatenate(
+        jax.lax.all_to_all(
+            jnp.stack(jnp.split(out_columns, jax.lax.axis_size("ep"), 0), 0), "ep", 0, 0
+        ),
+        1,
+    )
     hidden = layer_norm(
         residual_scale * sequence_input_rows.astype(jnp.float32) + attn_out.astype(jnp.float32),
         mixer_norm_gain,

time: 139 us -> 148 us (1.065)
  local copies, waits for them, and re-layouts: 11 us -> 19.7 us
    unnamed x22 -> x37, local copies, waits for them, and re-layouts: 4.3 us -> 13 us
where the time goes in v1:
time: 148 us; the launch traced here: 147 us
  blocking collectives  48.2 us (33%)
  matrix products  30.5 us (21%)
  waiting for transfers between devices  21.7 us (15%)
  local copies, waits for them, and re-layouts  19.7 us (13%)
  starting transfers between devices  14.2 us (10%)
  other arithmetic  12 us (8%)
    all_gather x1, blocking collectives, on_device(): section = lax.all_gather(sequence_input_rows, 'ep', axis=0, tiled=True)  25 us
    all_gather x1, blocking collectives, on_device(): lax.all_gather(attention_mixing_outcome, 'ep', axis=0, tiled=True)  23.2 us
    dot_general x1, matrix products, token_mixer_step(): jnp.einsum('bhvk,bhk->bhv', value_key_state, removal_dir, precision=lax.P...  13.6 us
    unnamed x37, local copies, waits for them, and re-layouts  13 us
    add x1, other arithmetic, token_mixer_step(): value_key_state * decay_heads[:, :, None, :]  7.89 us
    all_to_all x1, waiting for transfers between devices, by_exchange(): lax.all_to_all(finished, 'ep', split_axis=0, concat_axis=0, tiled=True)  7.72 us
    all_to_all x1, waiting for transfers between devices, by_exchange(): lax.all_to_all(outgoing, 'ep', split_axis=0, concat_axis=0, tiled=True)  7.39 us
    all_to_all x1, waiting for transfers between devices, on_device(): jax.lax.all_to_all(jnp.stack(jnp.split(out_columns, jax.lax.axis_size('ep...  6.58 us
  transfers between devices with their start and end apart: 4, of which 3 were waited for; matrix products, arithmetic and copies ran while one was open for 6% of the time, Pallas kernels for 0%

profile of v1, /device:TPU:0, one launch (start us, length us, event | category | flops | bytes accessed | tf_op | source)
XLA Modules:
  0.0 147.2 jit_solution(13530235959871318910)
XLA Ops:
  0.6 25.0 %all-gather = bf16[16,7,2048]{2,1,0:T(8,128)(2,1)S(1)} all-gather(bf16[1,7,2048]{2,1,0:T(8,128)(2,1)} %bitcast.165), channel_id=1, replica_groups=mesh['grp'=2,'ep'=16] {'ep'}, dimensions={0}, use_global_device_ids=true | all-gather | bytes 487424 | tf_op jit(solution)/shard_map/all_gather | solution.py:193
  25.8 1.3 fusion.10
  27.1 1.3 fusion.11
  28.4 1.3 fusion.9
  29.7 0.7 copy.40
  30.4 3.5 %all-to-all-start = ((bf16[112,3,128]{2,1,0:T(4,128)(2,1)}), bf16[112,3,128]{2,1,0:T(4,128)(2,1)S(1)}, u32[]{:S(2)}, u32[]{:S(2)}) async-start(bf16[112,3,128]{2,1,0:T(4,128)(2,1)} %copy.40), calls=%async_computation | async-start | bytes 229376 | tf_op jit(solution)/shard_map/all_to_all | solution.py:199
  34.0 0.8 copy.43
  35.1 1.4 fusion.4
  36.6 1.5 %fusion.24 = f32[7,2048]{1,0:T(8,128)S(1)} fusion(bf16[64,2048]{1,0:T(8,128)(2,1)} %param.30, bf16[7,2048]{1,0:T(8,128)(2,1)} %param.24, bf16[2048,64]{0,1:T(8,128)(2,1)} %param.29, f32[2048]{0:T(1024)} %param.31), kind=kOutput, calls=%fused_computation.45 | convolution fusion | flops 3828160 | bytes 618496 | tf_op jit(solution)/shard_map/dot_general | solution.py:40
  38.1 0.8 slice_bitcast_fusion.18
  38.9 0.8 mul.214
  39.8 0.8 mul.225
  40.6 0.8 mul.233
  42.2 13.6 %fusion.48 = f32[7,32,1,64]{3,2,1,0:T(1,128)S(1)} fusion(f32[7,32,64,1]{2,3,1,0:T(1,128)S(1)} %bitcast.168, f32[7,32,64,64]{3,2,1,0:T(8,128)} %param.25), kind=kOutput, calls=%fused_computation.166 | convolution fusion | flops 11010048 | bytes 3784704 | tf_op jit(solution)/shard_map/bhvk,bhk->bhv/dot_general | solution.py:74
  55.9 7.9 %multiply_add_fusion = f32[7,32,64,64]{3,2,1,0:T(8,128)S(1)} fusion(f32[7,32,64,64]{3,2,1,0:T(8,128)} %param.25, f32[7,32,64]{2,1,0:T(8,128)S(1)} %get-tuple-element.15, f32[7,32,64]{2,1,0:T(8,128)S(1)} %reshape.447, f32[7,32,64]{2,1,0:T(8,128)S(1)} %get-tuple-element.13, f32[7,32,64]{2,1,0:T(8,128)S(1)} %bitcast.167, f32[7,32,64]{2,1,0:T(8,128)S(1)} %mul.211), kind=kLoop, calls=%fused_computation.2 | loop fusion | flops 4587520 | bytes 7626752 | tf_op jit(solution)/shard_map/add | solution.py:78
  63.8 3.0 %copy-done.1 = f32[7,32,64,64]{3,2,1,0:T(8,128)} copy-done((f32[7,32,64,64]{3,2,1,0:T(8,128)}, f32[7,32,64,64]{3,2,1,0:T(8,128)S(1)}, u32[]{:S(2)}) %copy-start.1) | copy-done | bytes 3670040
  66.9 5.8 %fusion.49 = f32[7,32,1,64]{3,2,1,0:T(1,128)S(1)} fusion(f32[7,32,64,64]{3,2,1,0:T(8,128)S(1)} %multiply_add_fusion, bf16[7,32,64,1]{2,3,1,0:T(2,128)(2,1)S(1)} %reshape.482), kind=kOutput, calls=%fused_computation.167 | convolution fusion | flops 11010048 | bytes 3756032 | tf_op jit(solution)/shard_map/bhvk,bhk->bhv/dot_general | solution.py:82
  73.0 0.5 fusion.8
  73.6 23.2 %all-gather.1 = bf16[16,7,2048]{2,1,0:T(8,128)(2,1)S(1)} all-gather(bf16[1,7,2048]{2,1,0:T(8,128)(2,1)S(1)} %reshape.474), channel_id=1, replica_groups=mesh['grp'=2,'ep'=16] {'ep'}, dimensions={0}, use_global_device_ids=true | all-gather | bytes 487424 | tf_op jit(solution)/shard_map/all_gather | solution.py:218
  97.0 1.3 convolution_convert_fusion.2
  98.3 0.6 constant_dynamic-update-slice_fusion.15
  98.9 0.6 constant_dynamic-update-slice_fusion.14
  99.4 0.6 constant_dynamic-update-slice_fusion.13
  100.0 0.6 constant_dynamic-update-slice_fusion.12
  100.6 0.6 constant_dynamic-update-slice_fusion.11
  101.2 0.6 constant_dynamic-update-slice_fusion.10
  101.8 0.6 constant_dynamic-update-slice_fusion.9
  102.4 0.6 constant_dynamic-update-slice_fusion.8
  102.9 0.6 constant_dynamic-update-slice_fusion.7
  103.5 0.6 constant_dynamic-update-slice_fusion.6
  104.1 0.6 constant_dynamic-update-slice_fusion.5
  104.7 0.6 constant_dynamic-update-slice_fusion.4
  105.3 0.6 constant_dynamic-update-slice_fusion.3
  105.8 0.6 constant_dynamic-update-slice_fusion.2
  106.4 0.6 constant_dynamic-update-slice_fusion.1
  107.0 0.6 constant_dynamic-update-slice_fusion
  107.6 3.7 %all-to-all-start.1 = ((bf16[16,7,128]{2,1,0:T(8,128)(2,1)}), bf16[16,7,128]{2,1,0:T(8,128)(2,1)S(1)}, u32[]{:S(2)}, u32[]{:S(2)}) async-start(bf16[16,7,128]{2,1,0:T(8,128)(2,1)} %constant_dynamic-update-slice_fusion), calls=%async_computation.1 | async-start | bytes 65536 | tf_op jit(solution)/shard_map/all_to_all | solution.py:223
  111.3 6.6 %all-to-all-done.1 = bf16[16,7,128]{2,1,0:T(8,128)(2,1)S(1)} async-done(((bf16[16,7,128]{2,1,0:T(8,128)(2,1)}), bf16[16,7,128]{2,1,0:T(8,128)(2,1)S(1)}, u32[]{:S(2)}, u32[]{:S(2)}) %all-to-all-start.1) | async-done | bytes 28704 | tf_op jit(solution)/shard_map/all_to_all | solution.py:223
  118.6 0.7 reshape.442
  119.3 3.5 %all-to-all-start.2 = ((bf16[16,2,2048]{2,1,0:T(2,128)(2,1)}), bf16[16,2,2048]{2,1,0:T(2,128)(2,1)S(1)}, u32[]{:S(2)}, u32[]{:S(2)}) async-start(bf16[16,2,2048]{2,1,0:T(2,128)(2,1)} %reshape.442), calls=%async_computation.2 | async-start | bytes 262144 | tf_op jit(solution)/shard_map/all_to_all | solution.py:150
  123.3 7.4 %all-to-all-done.2 = bf16[16,2,2048]{2,1,0:T(2,128)(2,1)S(1)} async-done(((bf16[16,2,2048]{2,1,0:T(2,128)(2,1)}), bf16[16,2,2048]{2,1,0:T(2,128)(2,1)S(1)}, u32[]{:S(2)}, u32[]{:S(2)}) %all-to-all-start.2) | async-done | bytes 131104 | tf_op jit(solution)/shard_map/all_to_all | solution.py:150
  130.7 1.5 %fusion.17 = f32[32,256]{1,0:T(8,128)S(1)} fusion(bf16[32,2048]{1,0:T(8,128)(2,1)S(1)} %reshape.443, bf16[1,2048,256]{2,1,0:T(8,128)(2,1)} %param.43), kind=kOutput, calls=%fused_computation.29 | convolution fusion | flops 33554432 | bytes 1212416 | tf_op jit(solution)/shard_map/dot_general | solution.py:131
  132.3 0.7 convolution_convert_fusion
  133.0 0.8 reshape.444
  133.8 3.5 %all-to-all-start.3 = ((bf16[16,2,2048]{2,1,0:T(2,128)(2,1)}), bf16[16,2,2048]{2,1,0:T(2,128)(2,1)S(1)}, u32[]{:S(2)}, u32[]{:S(2)}) async-start(bf16[16,2,2048]{2,1,0:T(2,128)(2,1)} %reshape.444), calls=%async_computation.3 | async-start | bytes 262144 | tf_op jit(solution)/shard_map/all_to_all | solution.py:153
  137.4 7.7 %all-to-all-done.3 = bf16[16,2,2048]{2,1,0:T(2,128)(2,1)S(1)} async-done(((bf16[16,2,2048]{2,1,0:T(2,128)(2,1)}), bf16[16,2,2048]{2,1,0:T(2,128)(2,1)S(1)}, u32[]{:S(2)}, u32[]{:S(2)}) %all-to-all-start.3) | async-done | bytes 131104 | tf_op jit(solution)/shard_map/all_to_all | solution.py:153
  145.2 0.6 gather_fusion
  146.5 0.7 multiply_convert_fusion
  (65 shorter events, 4.2 us)
Async XLA Ops:
  0.6 131.6 %copy-start = (bf16[1,256,2048]{2,1,0:T(8,128)(2,1)S(1)}, bf16[1,256,2048]{2,1,0:T(8,128)(2,1)}, u32[]{:S(2)}) copy-start(bf16[1,256,2048]{2,1,0:T(8,128)(2,1)} %param.45) | copy-start | bytes 3145732
  30.4 11.1 %all-to-all-start = ((bf16[112,3,128]{2,1,0:T(4,128)(2,1)}), bf16[112,3,128]{2,1,0:T(4,128)(2,1)S(1)}, u32[]{:S(2)}, u32[]{:S(2)}) async-start(bf16[112,3,128]{2,1,0:T(4,128)(2,1)} %copy.40), calls=%async_computation | async-start | bytes 229376 | tf_op jit(solution)/shard_map/all_to_all | solution.py:199
  63.8 3.1 %copy-start.1 = (f32[7,32,64,64]{3,2,1,0:T(8,128)}, f32[7,32,64,64]{3,2,1,0:T(8,128)S(1)}, u32[]{:S(2)}) copy-start(f32[7,32,64,64]{3,2,1,0:T(8,128)S(1)} %multiply_add_fusion) | copy-start | bytes 11010052
  66.8 6.2 %copy-start.4 = (f32[32,64]{1,0:T(8,128)S(1)}, f32[32,64]{1,0:T(8,128)}, u32[]{:S(2)}) copy-start(f32[32,64]{1,0:T(8,128)} %param.37) | copy-start | bytes 24580
  66.8 51.0 %copy-start.2 = (bf16[7,2048]{1,0:T(8,128)(2,1)S(1)}, bf16[7,2048]{1,0:T(8,128)(2,1)}, u32[]{:S(2)}) copy-start(bf16[7,2048]{1,0:T(8,128)(2,1)} %param.24) | copy-start | bytes 86020
  66.8 51.4 %copy-start.6 = (f32[2048]{0:T(1024)S(1)}, f32[2048]{0:T(1024)}, u32[]{:S(2)}) copy-start(f32[2048]{0:T(1024)} %param.40) | copy-start | bytes 24580
  66.8 56.0 %copy-start.8 = (bf16[2048,4]{0,1:T(4,128)(2,1)S(1)}, bf16[2048,4]{0,1:T(4,128)(2,1)}, u32[]{:S(2)}) copy-start(bf16[2048,4]{0,1:T(4,128)(2,1)} %param.41) | copy-start | bytes 49156
  66.8 56.2 %copy-start.7 = (bf16[2048,16]{0,1:T(8,128)(2,1)S(1)}, bf16[2048,16]{0,1:T(8,128)(2,1)}, u32[]{:S(2)}) copy-start(bf16[2048,16]{0,1:T(8,128)(2,1)} %param.42) | copy-start | bytes 196612
  66.9 65.4 %copy-start.3 = (bf16[1,2048,256]{2,1,0:T(8,128)(2,1)S(1)}, bf16[1,2048,256]{2,1,0:T(8,128)(2,1)}, u32[]{:S(2)}) copy-start(bf16[1,2048,256]{2,1,0:T(8,128)(2,1)} %param.44) | copy-start | bytes 3145732
  72.7 73.8 %copy-start.5 = (f32[2048]{0:T(1024)S(1)}, f32[2048]{0:T(1024)}, u32[]{:S(2)}) copy-start(f32[2048]{0:T(1024)} %param.46) | copy-start | bytes 24580
  107.6 10.3 %all-to-all-start.1 = ((bf16[16,7,128]{2,1,0:T(8,128)(2,1)}), bf16[16,7,128]{2,1,0:T(8,128)(2,1)S(1)}, u32[]{:S(2)}, u32[]{:S(2)}) async-start(bf16[16,7,128]{2,1,0:T(8,128)(2,1)} %constant_dynamic-update-slice_fusion), calls=%async_computation.1 | async-start | bytes 65536 | tf_op jit(solution)/shard_map/all_to_all | solution.py:223
  119.3 11.4 %all-to-all-start.2 = ((bf16[16,2,2048]{2,1,0:T(2,128)(2,1)}), bf16[16,2,2048]{2,1,0:T(2,128)(2,1)S(1)}, u32[]{:S(2)}, u32[]{:S(2)}) async-start(bf16[16,2,2048]{2,1,0:T(2,128)(2,1)} %reshape.442), calls=%async_computation.2 | async-start | bytes 262144 | tf_op jit(solution)/shard_map/all_to_all | solution.py:150
  133.8 11.4 %all-to-all-start.3 = ((bf16[16,2,2048]{2,1,0:T(2,128)(2,1)}), bf16[16,2,2048]{2,1,0:T(2,128)(2,1)S(1)}, u32[]{:S(2)}, u32[]{:S(2)}) async-start(bf16[16,2,2048]{2,1,0:T(2,128)(2,1)} %reshape.444), calls=%async_computation.3 | async-start | bytes 262144 | tf_op jit(solution)/shard_map/all_to_all | solution.py:153
